TPU v7x, 512 devices: a 4x2x32 block of a 4x8x32 slice. The times are simulated.
512 devices in a mesh: grp: 2 (over y), fs: 32 (over z), tp: 8 (over x, core).
Axes of the slice: x: 4, y: 2, z: 32, core: 2. Of those that a mesh axis runs over, the one named last changes fastest.
The devices are a block of a 4x8x32 slice.
Arguments:
- stream: bfloat16 [64, 128, 2048], P(('grp', 'fs')), parts along dimension 0, may hold values from -6 to 6
- in_gain: float32 [2048], replicated, may hold values from 0.2 to 5
- value_weight: bfloat16 [2048, 1024], P('fs', 'tp'), may hold values from -0.125 to 0.125
- gate_weight: bfloat16 [2048, 1024], P('fs', 'tp'), may hold values from -0.125 to 0.125
- conv_kernel: bfloat16 [31, 1024], P(None, 'tp'), may hold values from -3.6 to 3.6
- conv_gain: float32 [1024], P('tp'), may hold values from 0.1 to 1.9
- conv_shift: float32 [1024], P('tp'), may hold values from -3 to 3
- out_weight: bfloat16 [1024, 2048], P('tp', 'fs'), may hold values from -0.1875 to 0.1875
- norm_gain: float32 [2048], replicated, may hold values from 0.2 to 5
- up_weight: bfloat16 [2048, 8192], P('fs', 'tp'), may hold values from -0.125 to 0.125
- down_weight: bfloat16 [8192, 2048], P('tp', 'fs'), may hold values from -0.0625 to 0.0625
- out_gain: float32 [2048], P('tp'), may hold values from 0.1 to 1.9
Outputs:
- result: bfloat16 [64, 128, 2048], P(('grp', 'fs'), None, 'tp'), parts along dimension 0
There are 2 independent parts, one for each index of `grp`. A program takes and returns all parts, laid end to end along the dimension named above; an argument that names none is the same for every part. Nothing has to cross between parts.
All inputs are finite; a program needn't handle non-finite values.
Results may differ from a plain program's by a relative error of at most 0.02.
Values may be sent and summed in bfloat16 or wider, within the bound.
No kernel may reach another device: no remote copies, remote signals or barrier semaphores. Data moves between devices by JAX's collectives and lax.ppermute only.
A program may use at most 64 MiB of HBM per device.

v0:
```python
import jax
import jax.numpy as jnp
from jax import lax
from jax.sharding import PartitionSpec as P

KW = 31
norm_epsilon = 1e-05
residual_scale = 2.0**0.25
feature_scale = 2.0**7


def to_half(x, scale):
    return (x.astype(jnp.float32) * scale).astype(jnp.float16)


def from_half(x, scale):
    return (x.astype(jnp.float32) * (1 / scale)).astype(jnp.bfloat16)


def gather_fs(x):
    return lax.all_gather(x, "fs", axis=0, tiled=True)


def in_order(is_even, mine, theirs):
    return (jnp.where(is_even, mine, theirs), jnp.where(is_even, theirs, mine))


def norm_rows(values, gain_vector):
    row_mean = jnp.mean(values, axis=-1, keepdims=True)
    row_var = jnp.mean(jnp.square(values - row_mean), axis=-1, keepdims=True)
    return (values - row_mean) * lax.rsqrt(row_var + norm_epsilon) * gain_vector


def contract(left, turned):
    return lax.dot_general(
        left, turned, (((1,), (1,)), ((), ())), preferred_element_type=jnp.float32
    )


def swap_blocks(x):
    return lax.all_to_all(x, "tp", 0, 0, tiled=True)


def summed(tiles):
    return jnp.sum(tiles.astype(jnp.float32), axis=0).astype(jnp.bfloat16)


def shards(
    stream,
    in_gain,
    value_weight,
    gate_weight,
    conv_kernel,
    conv_gain,
    conv_shift,
    out_weight,
    norm_gain,
    up_weight,
    down_weight,
    out_gain,
):
    seq_count, seq_length, model_width = stream.shape
    token_count = seq_count * seq_length
    tp_count = lax.axis_size("tp")
    group_count = lax.axis_size("grp")
    slice_width = model_width // tp_count
    own_tokens = token_count // tp_count
    tp_index = lax.axis_index("tp")
    channels = value_weight.shape[1]
    sharing = 2 if group_count % 2 == 0 else 1
    partner = [(g, g ^ 1) for g in range(group_count)]
    is_even = lax.axis_index("grp") % 2 == 0
    teams = [
        [g * tp_count + t for t in range(tp_count) for g in range(first, first + sharing)]
        for first in range(0, group_count, sharing)
    ]
    share = up_weight.shape[1] // sharing
    up_shard, down_shard = (up_weight, down_weight.T)
    if sharing == 2:
        up_shard = jnp.where(is_even, up_shard[:, :share], up_shard[:, share:])
        down_shard = jnp.where(is_even, down_shard[:, :share], down_shard[:, share:])
    feed = gather_fs(jnp.concatenate([up_shard, down_shard], axis=1))
    up_whole, down_turned = (feed[:, :share], feed[:, share:])
    rows = value_weight.shape[0]
    half = rows // 2
    out_shard = out_weight.T
    even_part = jnp.concatenate([value_weight, out_shard[:half]], axis=0)
    odd_part = jnp.concatenate([gate_weight, out_shard[half:]], axis=0)
    if sharing == 2:
        mine = gather_fs(jnp.where(is_even, even_part, odd_part))
        theirs = lax.ppermute(mine, "grp", partner)
        even_whole, odd_whole = in_order(is_even, mine, theirs)
    else:
        even_whole, odd_whole = (gather_fs(even_part), gather_fs(odd_part))
    even_whole = even_whole.reshape(-1, rows + half, channels)
    odd_whole = odd_whole.reshape(-1, rows + half, channels)
    value_whole = even_whole[:, :rows].reshape(-1, channels)
    gate_whole = odd_whole[:, :rows].reshape(-1, channels)
    out_turned = jnp.concatenate([even_whole[:, rows:], odd_whole[:, rows:]], axis=1).reshape(
        -1, channels
    )
    normed = norm_rows(
        stream.reshape(token_count, model_width).astype(jnp.float32), in_gain
    ).astype(jnp.bfloat16)
    values = jnp.dot(normed, value_whole, preferred_element_type=jnp.float32)
    gating = jnp.dot(normed, gate_whole, preferred_element_type=jnp.float32)
    gated = (values * jax.nn.sigmoid(gating)).astype(jnp.bfloat16)
    convolved = lax.conv_general_dilated(
        gated.reshape(seq_count, seq_length, channels),
        conv_kernel[:, None, :],
        window_strides=(1,),
        padding=[(KW - 1, 0)],
        dimension_numbers=("NWC", "WIO", "NWC"),
        feature_group_count=channels,
        preferred_element_type=jnp.float32,
    ).reshape(token_count, channels)
    told = jnp.concatenate(
        [jnp.sum(convolved, axis=1), jnp.sum(convolved * convolved, axis=1), out_gain]
    )
    normed_own = lax.dynamic_slice_in_dim(normed, tp_index * own_tokens, own_tokens, 0)
    told, out_turned, normed_own, norm_gain = lax.optimization_barrier(
        (told, out_turned, normed_own, norm_gain)
    )
    heard = swap_blocks(jnp.broadcast_to(told[None], (tp_count, *told.shape)))
    sums = jnp.sum(heard[:, : 2 * token_count], axis=0).reshape(2, token_count)
    whole_gain = heard[:, 2 * token_count :].reshape(model_width)
    row_mean = sums[0] / (channels * tp_count)
    row_var = sums[1] / (channels * tp_count) - row_mean * row_mean
    activated = jax.nn.silu(
        (convolved - row_mean[:, None]) * lax.rsqrt(row_var + norm_epsilon)[:, None] * conv_gain
        + conv_shift
    ).astype(jnp.bfloat16)
    mixed_terms = contract(activated, out_turned).astype(jnp.bfloat16)
    mixed_terms, whole_gain = lax.optimization_barrier((mixed_terms, whole_gain))
    mixed = summed(swap_blocks(mixed_terms.reshape(tp_count, own_tokens, model_width)))
    settled_own = norm_rows(
        residual_scale * normed_own.astype(jnp.float32) + mixed.astype(jnp.float32), norm_gain
    ).astype(jnp.bfloat16)
    if sharing == 2:
        their_settled = lax.ppermute(settled_own, "grp", partner)
        pair_settled = jnp.stack(in_order(is_even, settled_own, their_settled))
    else:
        pair_settled = settled_own[None]
    settled = from_half(
        lax.all_gather(to_half(pair_settled, feature_scale), "tp", axis=0, tiled=True),
        feature_scale,
    ).reshape(sharing * token_count, model_width)
    hidden = jnp.square(
        jax.nn.relu(jnp.dot(settled, up_whole, preferred_element_type=jnp.float32))
    ).astype(jnp.bfloat16)
    hidden = lax.optimization_barrier(hidden)
    fed_terms = contract(hidden, down_turned).astype(jnp.bfloat16)
    fed = summed(
        lax.all_to_all(
            fed_terms.reshape(sharing * tp_count, own_tokens, model_width),
            ("grp", "tp"),
            0,
            0,
            tiled=True,
            axis_index_groups=teams,
        )
    )
    result_own = norm_rows(
        residual_scale * settled_own.astype(jnp.float32) + fed.astype(jnp.float32), whole_gain
    ).astype(jnp.bfloat16)
    pieces = jnp.moveaxis(result_own.reshape(own_tokens, tp_count, slice_width), 1, 0)
    return swap_blocks(pieces).reshape(seq_count, seq_length, slice_width)


def solution(mesh):
    in_specs = (
        P(("grp", "fs"), None, None),
        P(),
        P("fs", "tp"),
        P("fs", "tp"),
        P(None, "tp"),
        P("tp"),
        P("tp"),
        P("tp", "fs"),
        P(),
        P("fs", "tp"),
        P("tp", "fs"),
        P("tp"),
    )
    out_specs = P(("grp", "fs"), None, "tp")
    return jax.shard_map(shards, mesh=mesh, in_specs=in_specs, out_specs=out_specs, check_vma=False)
```

profile of v0, /device:TPU:33, one launch (start us, length us, event | category | flops | bytes accessed | tf_op | source)
XLA Modules:
  0.0 217.8 jit_solution(2617139166442563405)
XLA Ops:
  6.5 0.0 copy-start
  6.6 1.0 slice_select_fusion
  7.6 0.7 pad_maximum_fusion.1
  8.2 0.1 all-gather.3.cloned.1.call-update
  8.3 0.7 fusion.37
  9.0 0.7 maximum_select_fusion
  9.8 89.2 %all_gather.9 = bf16[3072,128]{1,0:T(8,128)(2,1)S(1)} all-gather(bf16[96,128]{1,0:T(8,128)(2,1)S(1)} %maximum_select_fusion), channel_id=1, replica_groups=mesh['grp'=2,'fs'=32,'tp'=8] {'fs'}, dimensions={0}, use_global_device_ids=true | all-gather | bytes 811008 | tf_op jit(solution)/shard_map/all_gather | solution.py:21
  98.9 6.8 %collective-permute-start = (bf16[3072,128]{1,0:T(8,128)(2,1)S(1)}, bf16[3072,128]{1,0:T(8,128)(2,1)S(1)}, u32[]{:S(2)}, u32[]{:S(2)}) collective-permute-start(bf16[3072,128]{1,0:T(8,128)(2,1)S(1)} %all_gather.9), channel_id=1, source_target_pairs={{0,256},{256,0},{1,257},{257,1},{2,258},{258,2},{3,259},{259,3},{4... | collective-permute-start | bytes 2359304 | tf_op jit(solution)/shard_map/ppermute | solution.py:91
  105.8 0.0 copy-done.1
  105.8 0.2 convert_reduce_fusion
  106.0 0.3 fusion.20
  106.3 0.1 dynamic-slice
  106.3 0.1 fusion.23
  106.4 9.1 %collective-permute-done = bf16[3072,128]{1,0:T(8,128)(2,1)S(1)} collective-permute-done((bf16[3072,128]{1,0:T(8,128)(2,1)S(1)}, bf16[3072,128]{1,0:T(8,128)(2,1)S(1)}, u32[]{:S(2)}, u32[]{:S(2)}) %collective-permute-start) | collective-permute-done | bytes 786464 | tf_op jit(solution)/shard_map/ppermute | solution.py:91
  115.6 0.1 broadcast_select_fusion.1
  115.7 0.1 slice.69
  115.8 0.1 slice.68
  115.9 0.0 copy-start.4
  115.9 0.4 fusion.14
  116.3 0.0 copy-start.5
  116.3 0.0 copy-start.6
  116.3 0.4 fusion.16
  116.7 1.1 fusion.38
  117.8 0.1 multiply_reduce_fusion.3
  117.9 0.0 copy-start.3
  117.9 0.1 pad_maximum_fusion
  118.0 20.6 %all_to_all.24 = f32[8,1,512]{2,1,0:T(1,128)S(1)} all-to-all(f32[8,1,512]{2,1,0:T(1,128)S(1)} %broadcast_in_dim.5), channel_id=1, replica_groups=mesh['grp'=2,'fs'=32,'tp'=8] {'tp'}, dimensions={0} | all-to-all | bytes 32768 | tf_op jit(solution)/shard_map/all_to_all | solution.py:41
  138.6 0.4 convolution_convert_fusion.1
  139.0 12.5 %all_to_all.25 = bf16[8,16,2048]{2,1,0:T(8,128)(2,1)S(1)} all-to-all(bf16[8,16,2048]{2,1,0:T(8,128)(2,1)S(1)} %bitcast.53), channel_id=1, replica_groups=mesh['grp'=2,'fs'=32,'tp'=8] {'tp'}, dimensions={0} | all-to-all | bytes 1048576 | tf_op jit(solution)/shard_map/all_to_all | solution.py:41
  151.5 0.1 reduce_sum.110
  151.6 0.1 fusion.24
  151.7 0.2 multiply_reduce_fusion.2
  152.0 0.1 multiply_convert_fusion.3
  152.1 3.7 %collective-permute-start.1 = (bf16[16,2048]{1,0:T(8,128)(2,1)S(1)}, bf16[16,2048]{1,0:T(8,128)(2,1)S(1)}, u32[]{:S(2)}, u32[]{:S(2)}) collective-permute-start(bf16[16,2048]{1,0:T(8,128)(2,1)S(1)} %multiply_convert_fusion.3), channel_id=1, source_target_pairs={{0,256},{256,0},{1,257},{257,1},{2,258},{258,2},{3,259},{259,3},{4... | collective-permute-start | bytes 196616 | tf_op jit(solution)/shard_map/ppermute | solution.py:140
  155.8 2.0 collective-permute-done.1
  157.9 15.3 %all-gather.4 = f16[16,16,2048]{2,1,0:T(8,128)(2,1)S(1)} all-gather(f16[2,16,2048]{2,1,0:T(8,128)(2,1)S(1)} %multiply_convert_fusion.1), channel_id=1, replica_groups=mesh['grp'=2,'fs'=32,'tp'=8] {'tp'}, dimensions={0}, use_global_device_ids=true | all-gather | bytes 1179648 | tf_op jit(solution)/shard_map/all_gather | solution.py:145
  173.1 0.2 multiply_convert_fusion
  173.3 0.0 all-gather.3.cloned.1.call-done
  173.4 2.4 %fusion.9 = bf16[256,512]{1,0:T(8,128)(2,1)S(1)} fusion(bf16[256,2048]{1,0:T(8,128)(2,1)S(1)} %bitcast.54, bf16[2048,1024]{1,0:T(8,128)(2,1)} %all-gather.3.cloned.1.call-done), kind=kOutput, calls=%fused_computation.11 | convolution fusion | flops 537264128 | bytes 3407872 | tf_op jit(solution)/shard_map/dot_general | solution.py:149
  175.8 0.4 copy-done.7
  176.2 0.7 convolution_convert_fusion
  176.9 24.6 %all_to_all.26 = bf16[16,16,2048]{2,1,0:T(8,128)(2,1)S(1)} all-to-all(bf16[16,16,2048]{2,1,0:T(8,128)(2,1)S(1)} %bitcast.55), channel_id=1, replica_groups={{0,256,1,257,2,258,3,259,4,260,5,261,6,262,7,263},{8,264,9,265,10,266,1..., dimensions={0} | all-to-all | bytes 2097152 | tf_op jit(solution)/shard_map/all_to_all | solution.py:154
  201.5 0.1 reduce_sum.113
  201.7 0.1 fusion.25
  201.8 0.2 multiply_reduce_fusion.1
  202.0 0.1 multiply_convert_fusion.2
  202.1 8.1 %all_to_all.27 = bf16[8,16,256]{2,1,0:T(8,128)(2,1)S(1)} all-to-all(bf16[8,16,256]{2,1,0:T(8,128)(2,1)S(1)} %bitcast.61), channel_id=1, replica_groups=mesh['grp'=2,'fs'=32,'tp'=8] {'tp'}, dimensions={0} | all-to-all | bytes 131072 | tf_op jit(solution)/shard_map/all_to_all | solution.py:41
  210.3 0.6 copy.44
  (27 shorter events, 0.2 us)
Async XLA Ops:
  6.5 110.1 %copy-start = (bf16[31,128]{1,0:T(8,128)(2,1)S(1)}, bf16[31,128]{1,0:T(8,128)(2,1)}, u32[]{:S(2)}) copy-start(bf16[31,128]{1,0:T(8,128)(2,1)} %param.16) | copy-start | bytes 23812
  6.6 99.2 %copy-start.1 = (bf16[1,128,2048]{2,1,0:T(8,128)(2,1)S(1)}, bf16[1,128,2048]{2,1,0:T(8,128)(2,1)}, u32[]{:S(2)}) copy-start(bf16[1,128,2048]{2,1,0:T(8,128)(2,1)} %param.12) | copy-start | bytes 1572868
  6.6 99.8 %copy-start.2 = (f32[2048]{0:T(1024)S(1)}, f32[2048]{0:T(1024)}, u32[]{:S(2)}) copy-start(f32[2048]{0:T(1024)} %param.13) | copy-start | bytes 24580
  6.6 166.8 %all-gather.3.cloned.1.call-start = ((), (), s32[]{:S(2)}) async-start(), calls=%async_computation.4 | async-start | bytes 4325376 | tf_op jit(solution)/shard_map/all_gather | solution.py:21
  98.9 16.6 %collective-permute-start = (bf16[3072,128]{1,0:T(8,128)(2,1)S(1)}, bf16[3072,128]{1,0:T(8,128)(2,1)S(1)}, u32[]{:S(2)}, u32[]{:S(2)}) collective-permute-start(bf16[3072,128]{1,0:T(8,128)(2,1)S(1)} %all_gather.9), channel_id=1, source_target_pairs={{0,256},{256,0},{1,257},{257,1},{2,258},{258,2},{3,259},{259,3},{4... | collective-permute-start | bytes 2359304 | tf_op jit(solution)/shard_map/ppermute | solution.py:91
  115.9 2.0 copy-start.4
  116.3 22.4 %copy-start.5 = (f32[128]{0:T(128)S(1)}, f32[128]{0:T(128)}, u32[]{:S(2)}) copy-start(f32[128]{0:T(128)} %param.18) | copy-start | bytes 1540
  116.3 22.4 %copy-start.6 = (f32[128]{0:T(128)S(1)}, f32[128]{0:T(128)}, u32[]{:S(2)}) copy-start(f32[128]{0:T(128)} %param.17) | copy-start | bytes 1540
  117.9 34.1 %copy-start.3 = (f32[2048]{0:T(1024)S(1)}, f32[2048]{0:T(1024)}, u32[]{:S(2)}) copy-start(f32[2048]{0:T(1024)} %param.20) | copy-start | bytes 24580
  152.1 5.7 %collective-permute-start.1 = (bf16[16,2048]{1,0:T(8,128)(2,1)S(1)}, bf16[16,2048]{1,0:T(8,128)(2,1)S(1)}, u32[]{:S(2)}, u32[]{:S(2)}) collective-permute-start(bf16[16,2048]{1,0:T(8,128)(2,1)S(1)} %multiply_convert_fusion.3), channel_id=1, source_target_pairs={{0,256},{256,0},{1,257},{257,1},{2,258},{258,2},{3,259},{259,3},{4... | collective-permute-start | bytes 196616 | tf_op jit(solution)/shard_map/ppermute | solution.py:140
  173.4 2.8 %copy-start.7 = (bf16[2048,1024]{1,0:T(8,128)(2,1)S(1)}, bf16[2048,1024]{1,0:T(8,128)(2,1)}, u32[]{:S(2)}) copy-start(bf16[2048,1024]{1,0:T(8,128)(2,1)} %all-gather.3.cloned.1.call-done) | copy-start | bytes 12582916
Sparse Core Ops, SparseCore 0:
  9.4 148.0 all-gather.2
where the time goes:
time: 218 us
  blocking collectives  170 us (78%)
  between operations  13.7 us (6%)
  waiting for transfers between devices  11.2 us (5%)
  starting transfers between devices  10.5 us (5%)
  matrix products  5.42 us (2%)
  other arithmetic  4.64 us (2%)
    all_gather x1, blocking collectives, gather_fs(): return lax.all_gather(x, 'fs', axis=0, tiled=True)  89.2 us
    all_to_all x3, blocking collectives, swap_blocks(): return lax.all_to_all(x, 'tp', 0, 0, tiled=True)  41.2 us
    all_to_all x1, blocking collectives, shards(): lax.all_to_all(fed_terms.reshape(sharing * tp_count, own_tokens, model_wi...  24.6 us
    all_gather x1, blocking collectives, shards(): lax.all_gather(to_half(pair_settled, feature_scale), 'tp', axis=0, tiled=...  15.3 us
    ppermute x1, waiting for transfers between devices, shards(): theirs = lax.ppermute(mine, 'grp', partner)  9.12 us
    ppermute x1, starting transfers between devices, shards(): theirs = lax.ppermute(mine, 'grp', partner)  6.85 us
  transfers between devices with their start and end apart: 3, of which 2 were waited for; matrix products, arithmetic and copies ran while one was open for 3% of the time, Pallas kernels for 0%

commit v1 on v0

--- a/solution.py
+++ b/solution.py
@@ -7,6 +7,21 @@
 norm_epsilon = 1e-05
 residual_scale = 2.0**0.25
 feature_scale = 2.0**7
+
+
+def _place_yards(work_x, along_dim):
+    nodes = lax.psum(1, "tp")
+    inbox = tuple(((ix, (ix + 1) % nodes) for ix in range(nodes)))
+    pieces_in = tuple(((ix, (ix - 1) % nodes) for ix in range(nodes)))
+    current_value, carry_out = ([work_x], [work_x])
+    for _ in range(nodes // 2):
+        current_value.append(lax.ppermute(current_value[-1], "tp", inbox))
+    for _ in range((nodes - 1) // 2):
+        z_new = lax.ppermute(carry_out[-1], "tp", pieces_in)
+        carry_out.append(z_new)
+    b_now = jnp.concatenate([*current_value[::-1], *carry_out[1:]], axis=along_dim)
+    frame_out = lax.axis_index("tp")
+    return jnp.roll(b_now, (frame_out - nodes // 2) * work_x.shape[along_dim], axis=along_dim)
 
 
 def to_half(x, scale):
@@ -142,8 +157,7 @@
     else:
         pair_settled = settled_own[None]
     settled = from_half(
-        lax.all_gather(to_half(pair_settled, feature_scale), "tp", axis=0, tiled=True),
-        feature_scale,
+        _place_yards(to_half(pair_settled, feature_scale), along_dim=0), feature_scale
     ).reshape(sharing * token_count, model_width)
     hidden = jnp.square(
         jax.nn.relu(jnp.dot(settled, up_whole, preferred_element_type=jnp.float32))

time: 218 us -> 278 us (1.28)
  waiting for transfers between devices: 11.2 us -> 59.7 us
  starting transfers between devices: 10.5 us -> 20.8 us
    all_gather x1, waiting for transfers between devices: 0.02 us -> 43.5 us  [gather_fs(): return lax.all_gather(x, 'fs', axis=0, tiled=True)]
    all_to_all x1, blocking collectives: 24.6 us -> 40.2 us  [shards(): lax.all_to_all(fed_terms.reshape(sharing * tp_count, own_tokens, model_wi...]
    all_gather x1 -> x0, blocking collectives: 15.3 us -> none  [shards(): lax.all_gather(to_half(pair_settled, feature_scale), 'tp', axis=0, tiled=...]
    ppermute x0 -> x7, starting transfers between devices: none -> 13.5 us  [the longest x4 7.98 us: _place_yards(): current_value.append(lax.ppermute(current_value[-1], 'tp', inbox))]
    ppermute x0 -> x7, waiting for transfers between devices: none -> 6.78 us  [the longest x4 4.55 us: _place_yards(): current_value.append(lax.ppermute(current_value[-1], 'tp', inbox))]
    all_to_all x3, blocking collectives: 41.2 us -> 44.4 us  [swap_blocks(): return lax.all_to_all(x, 'tp', 0, 0, tiled=True)]
    ppermute x1, starting transfers between devices: 6.85 us -> 3.77 us  [shards(): theirs = lax.ppermute(mine, 'grp', partner)]
  transfers between devices with their start and end apart: 3 -> 10, of which waited for: 2 -> 10; matrix products, arithmetic and copies ran while one was open for 3% -> 2% of each run, Pallas kernels for 0% -> 0%
where the time goes in v1:
time: 278 us
  blocking collectives  171 us (62%)
  waiting for transfers between devices  59.7 us (21%)
  starting transfers between devices  20.8 us (7%)
  between operations  13.8 us (5%)
  matrix products  5.4 us (2%)
  other arithmetic  4.67 us (2%)
    all_gather x1, blocking collectives, gather_fs(): return lax.all_gather(x, 'fs', axis=0, tiled=True)  86.5 us
    all_to_all x3, blocking collectives, swap_blocks(): return lax.all_to_all(x, 'tp', 0, 0, tiled=True)  44.4 us
    all_gather x1, waiting for transfers between devices, gather_fs(): return lax.all_gather(x, 'fs', axis=0, tiled=True)  43.5 us
    all_to_all x1, blocking collectives, shards(): lax.all_to_all(fed_terms.reshape(sharing * tp_count, own_tokens, model_wi...  40.2 us
    ppermute x4, starting transfers between devices, _place_yards(): current_value.append(lax.ppermute(current_value[-1], 'tp', inbox))  7.98 us
    ppermute x1, waiting for transfers between devices, shards(): theirs = lax.ppermute(mine, 'grp', partner)  7.34 us
  transfers between devices with their start and end apart: 10, of which 10 were waited for; matrix products, arithmetic and copies ran while one was open for 2% of the time, Pallas kernels for 0%

profile of v1, /device:TPU:33, one launch (start us, length us, event | category | flops | bytes accessed | tf_op | source)
XLA Modules:
  0.0 277.9 jit_solution(8868673079567310223)
XLA Ops:
  6.6 0.8 fusion.37
  7.3 0.7 maximum_select_fusion
  8.1 86.5 %all_gather.6 = bf16[3072,128]{1,0:T(8,128)(2,1)S(1)} all-gather(bf16[96,128]{1,0:T(8,128)(2,1)S(1)} %maximum_select_fusion), channel_id=1, replica_groups=mesh['grp'=2,'fs'=32,'tp'=8] {'fs'}, dimensions={0}, use_global_device_ids=true | all-gather | bytes 811008 | tf_op jit(solution)/shard_map/all_gather | solution.py:36
  94.6 3.8 %collective-permute-start = (bf16[3072,128]{1,0:T(8,128)(2,1)S(1)}, bf16[3072,128]{1,0:T(8,128)(2,1)S(1)}, u32[]{:S(2)}, u32[]{:S(2)}) collective-permute-start(bf16[3072,128]{1,0:T(8,128)(2,1)S(1)} %all_gather.6), channel_id=1, source_target_pairs={{0,256},{256,0},{1,257},{257,1},{2,258},{258,2},{3,259},{259,3},{4... | collective-permute-start | bytes 2359304 | tf_op jit(solution)/shard_map/ppermute | solution.py:106
  98.4 1.0 slice_select_fusion
  99.3 0.7 pad_maximum_fusion.1
  100.0 0.2 convert_reduce_fusion
  100.2 0.3 fusion.20
  100.7 7.3 %collective-permute-done = bf16[3072,128]{1,0:T(8,128)(2,1)S(1)} collective-permute-done((bf16[3072,128]{1,0:T(8,128)(2,1)S(1)}, bf16[3072,128]{1,0:T(8,128)(2,1)S(1)}, u32[]{:S(2)}, u32[]{:S(2)}) %collective-permute-start) | collective-permute-done | bytes 786464 | tf_op jit(solution)/shard_map/ppermute | solution.py:106
  108.0 0.1 broadcast_select_fusion.1
  108.2 0.4 fusion.14
  108.7 0.4 fusion.16
  109.1 1.1 fusion.38
  110.2 0.1 multiply_reduce_fusion.3
  110.4 23.7 %all_to_all.24 = f32[8,1,512]{2,1,0:T(1,128)S(1)} all-to-all(f32[8,1,512]{2,1,0:T(1,128)S(1)} %broadcast_in_dim.5), channel_id=1, replica_groups=mesh['grp'=2,'fs'=32,'tp'=8] {'tp'}, dimensions={0} | all-to-all | bytes 32768 | tf_op jit(solution)/shard_map/all_to_all | solution.py:56
  134.2 0.4 convolution_convert_fusion.1
  134.6 12.6 %all_to_all.25 = bf16[8,16,2048]{2,1,0:T(8,128)(2,1)S(1)} all-to-all(bf16[8,16,2048]{2,1,0:T(8,128)(2,1)S(1)} %bitcast.53), channel_id=1, replica_groups=mesh['grp'=2,'fs'=32,'tp'=8] {'tp'}, dimensions={0} | all-to-all | bytes 1048576 | tf_op jit(solution)/shard_map/all_to_all | solution.py:56
  147.2 0.1 fusion.24
  147.4 0.2 multiply_reduce_fusion.2
  147.6 0.1 multiply_convert_fusion.3
  147.7 3.6 %collective-permute-start.1 = (bf16[16,2048]{1,0:T(8,128)(2,1)S(1)}, bf16[16,2048]{1,0:T(8,128)(2,1)S(1)}, u32[]{:S(2)}, u32[]{:S(2)}) collective-permute-start(bf16[16,2048]{1,0:T(8,128)(2,1)S(1)} %multiply_convert_fusion.3), channel_id=1, source_target_pairs={{0,256},{256,0},{1,257},{257,1},{2,258},{258,2},{3,259},{259,3},{4... | collective-permute-start | bytes 196616 | tf_op jit(solution)/shard_map/ppermute | solution.py:155
  151.3 2.0 collective-permute-done.1
  153.4 1.8 collective-permute-start.2
  155.2 1.9 collective-permute-done.2
  157.1 2.4 collective-permute-start.3
  159.6 1.0 collective-permute-start.6
  160.6 0.9 collective-permute-done.3
  161.5 2.4 collective-permute-start.4
  164.0 0.4 collective-permute-done.6
  164.4 1.8 collective-permute-start.7
  166.2 0.8 collective-permute-done.4
  167.0 1.3 collective-permute-start.5
  168.4 0.8 collective-permute-done.7
  169.2 2.6 collective-permute-start.8
  171.8 0.8 collective-permute-done.5
  172.9 1.0 collective-permute-done.8
  174.2 0.2 multiply_convert_fusion
  174.4 43.5 %all-gather.2.cloned.1.call-done = bf16[2048,1024]{1,0:T(8,128)(2,1)} async-done(((bf16[64,1024]{1,0:T(8,128)(2,1)}), bf16[2048,1024]{1,0:T(8,128)(2,1)}) %all-gather.2.cloned.1.call-update) | async-done | bytes 4194320 | tf_op jit(solution)/shard_map/all_gather | solution.py:36
  217.9 2.4 fusion.9
  220.4 0.4 copy-done.7
  220.8 0.8 convolution_convert_fusion
  221.5 40.2 %all_to_all.26 = bf16[16,16,2048]{2,1,0:T(8,128)(2,1)S(1)} all-to-all(bf16[16,16,2048]{2,1,0:T(8,128)(2,1)S(1)} %bitcast.55), channel_id=1, replica_groups={{0,256,1,257,2,258,3,259,4,260,5,261,6,262,7,263},{8,264,9,265,10,266,1..., dimensions={0} | all-to-all | bytes 2097152 | tf_op jit(solution)/shard_map/all_to_all | solution.py:168
  261.7 0.1 reduce_sum.113
  261.8 0.1 fusion.25
  262.0 0.2 multiply_reduce_fusion.1
  262.2 0.1 multiply_convert_fusion.2
  262.3 8.1 %all_to_all.27 = bf16[8,16,256]{2,1,0:T(8,128)(2,1)S(1)} all-to-all(bf16[8,16,256]{2,1,0:T(8,128)(2,1)S(1)} %bitcast.61), channel_id=1, replica_groups=mesh['grp'=2,'fs'=32,'tp'=8] {'tp'}, dimensions={0} | all-to-all | bytes 131072 | tf_op jit(solution)/shard_map/all_to_all | solution.py:56
  270.4 0.6 copy.53
  (56 shorter events, 1.1 us)
Async XLA Ops:
  6.5 102.6 %copy-start = (bf16[31,128]{1,0:T(8,128)(2,1)S(1)}, bf16[31,128]{1,0:T(8,128)(2,1)}, u32[]{:S(2)}) copy-start(bf16[31,128]{1,0:T(8,128)(2,1)} %param.16) | copy-start | bytes 23812
  6.6 93.5 %copy-start.1 = (bf16[1,128,2048]{2,1,0:T(8,128)(2,1)S(1)}, bf16[1,128,2048]{2,1,0:T(8,128)(2,1)}, u32[]{:S(2)}) copy-start(bf16[1,128,2048]{2,1,0:T(8,128)(2,1)} %param.12) | copy-start | bytes 1572868
  6.6 94.0 %copy-start.2 = (f32[2048]{0:T(1024)S(1)}, f32[2048]{0:T(1024)}, u32[]{:S(2)}) copy-start(f32[2048]{0:T(1024)} %param.13) | copy-start | bytes 24580
  6.6 211.4 %all-gather.2.cloned.1.call-start = ((), (), s32[]{:S(2)}) async-start(), calls=%async_computation.4 | async-start | bytes 4325376 | tf_op jit(solution)/shard_map/all_gather | solution.py:36
  94.6 13.4 %collective-permute-start = (bf16[3072,128]{1,0:T(8,128)(2,1)S(1)}, bf16[3072,128]{1,0:T(8,128)(2,1)S(1)}, u32[]{:S(2)}, u32[]{:S(2)}) collective-permute-start(bf16[3072,128]{1,0:T(8,128)(2,1)S(1)} %all_gather.6), channel_id=1, source_target_pairs={{0,256},{256,0},{1,257},{257,1},{2,258},{258,2},{3,259},{259,3},{4... | collective-permute-start | bytes 2359304 | tf_op jit(solution)/shard_map/ppermute | solution.py:106
  108.6 1.7 copy-start.4
  109.0 25.2 %copy-start.5 = (f32[128]{0:T(128)S(1)}, f32[128]{0:T(128)}, u32[]{:S(2)}) copy-start(f32[128]{0:T(128)} %param.18) | copy-start | bytes 1540
  109.0 25.2 %copy-start.6 = (f32[128]{0:T(128)S(1)}, f32[128]{0:T(128)}, u32[]{:S(2)}) copy-start(f32[128]{0:T(128)} %param.17) | copy-start | bytes 1540
  110.3 37.3 %copy-start.3 = (f32[2048]{0:T(1024)S(1)}, f32[2048]{0:T(1024)}, u32[]{:S(2)}) copy-start(f32[2048]{0:T(1024)} %param.20) | copy-start | bytes 24580
  147.7 5.7 %collective-permute-start.1 = (bf16[16,2048]{1,0:T(8,128)(2,1)S(1)}, bf16[16,2048]{1,0:T(8,128)(2,1)S(1)}, u32[]{:S(2)}, u32[]{:S(2)}) collective-permute-start(bf16[16,2048]{1,0:T(8,128)(2,1)S(1)} %multiply_convert_fusion.3), channel_id=1, source_target_pairs={{0,256},{256,0},{1,257},{257,1},{2,258},{258,2},{3,259},{259,3},{4... | collective-permute-start | bytes 196616 | tf_op jit(solution)/shard_map/ppermute | solution.py:155
  153.4 3.7 %collective-permute-start.2 = (f16[2,16,2048]{2,1,0:T(8,128)(2,1)S(1)}, f16[2,16,2048]{2,1,0:T(8,128)(2,1)S(1)}, u32[]{:S(2)}, u32[]{:S(2)}) collective-permute-start(f16[2,16,2048]{2,1,0:T(8,128)(2,1)S(1)} %multiply_convert_fusion.1), channel_id=1, source_target_pairs={{0,1},{1,2},{2,3},{3,4},{4,5},{5,6},{6,7},{7,0},{8,9},{9,10},{10,1... | collective-permute-start | bytes 393224 | tf_op jit(solution)/shard_map/ppermute | solution.py:18
  157.1 4.4 %collective-permute-start.3 = (f16[2,16,2048]{2,1,0:T(8,128)(2,1)S(1)}, f16[2,16,2048]{2,1,0:T(8,128)(2,1)S(1)}, u32[]{:S(2)}, u32[]{:S(2)}) collective-permute-start(f16[2,16,2048]{2,1,0:T(8,128)(2,1)S(1)} %collective-permute-done.2), channel_id=1, source_target_pairs={{0,1},{1,2},{2,3},{3,4},{4,5},{5,6},{6,7},{7,0},{8,9},{9,10},{10,1... | collective-permute-start | bytes 393224 | tf_op jit(solution)/shard_map/ppermute | solution.py:18
  159.6 4.8 %collective-permute-start.6 = (f16[2,16,2048]{2,1,0:T(8,128)(2,1)S(1)}, f16[2,16,2048]{2,1,0:T(8,128)(2,1)S(1)}, u32[]{:S(2)}, u32[]{:S(2)}) collective-permute-start(f16[2,16,2048]{2,1,0:T(8,128)(2,1)S(1)} %multiply_convert_fusion.1), channel_id=1, source_target_pairs={{0,7},{1,0},{2,1},{3,2},{4,3},{5,4},{6,5},{7,6},{8,15},{9,8},{10,9... | collective-permute-start | bytes 393224 | tf_op jit(solution)/shard_map/ppermute | solution.py:20
  161.5 5.5 %collective-permute-start.4 = (f16[2,16,2048]{2,1,0:T(8,128)(2,1)S(1)}, f16[2,16,2048]{2,1,0:T(8,128)(2,1)S(1)}, u32[]{:S(2)}, u32[]{:S(2)}) collective-permute-start(f16[2,16,2048]{2,1,0:T(8,128)(2,1)S(1)} %collective-permute-done.3), channel_id=1, source_target_pairs={{0,1},{1,2},{2,3},{3,4},{4,5},{5,6},{6,7},{7,0},{8,9},{9,10},{10,1... | collective-permute-start | bytes 393224 | tf_op jit(solution)/shard_map/ppermute | solution.py:18
  164.4 4.8 %collective-permute-start.7 = (f16[2,16,2048]{2,1,0:T(8,128)(2,1)S(1)}, f16[2,16,2048]{2,1,0:T(8,128)(2,1)S(1)}, u32[]{:S(2)}, u32[]{:S(2)}) collective-permute-start(f16[2,16,2048]{2,1,0:T(8,128)(2,1)S(1)} %collective-permute-done.6), channel_id=1, source_target_pairs={{0,7},{1,0},{2,1},{3,2},{4,3},{5,4},{6,5},{7,6},{8,15},{9,8},{10,9... | collective-permute-start | bytes 393224 | tf_op jit(solution)/shard_map/ppermute | solution.py:20
  167.0 5.6 %collective-permute-start.5 = (f16[2,16,2048]{2,1,0:T(8,128)(2,1)S(1)}, f16[2,16,2048]{2,1,0:T(8,128)(2,1)S(1)}, u32[]{:S(2)}, u32[]{:S(2)}) collective-permute-start(f16[2,16,2048]{2,1,0:T(8,128)(2,1)S(1)} %collective-permute-done.4), channel_id=1, source_target_pairs={{0,1},{1,2},{2,3},{3,4},{4,5},{5,6},{6,7},{7,0},{8,9},{9,10},{10,1... | collective-permute-start | bytes 393224 | tf_op jit(solution)/shard_map/ppermute | solution.py:18
  169.2 4.7 %collective-permute-start.8 = (f16[2,16,2048]{2,1,0:T(8,128)(2,1)S(1)}, f16[2,16,2048]{2,1,0:T(8,128)(2,1)S(1)}, u32[]{:S(2)}, u32[]{:S(2)}) collective-permute-start(f16[2,16,2048]{2,1,0:T(8,128)(2,1)S(1)} %collective-permute-done.7), channel_id=1, source_target_pairs={{0,7},{1,0},{2,1},{3,2},{4,3},{5,4},{6,5},{7,6},{8,15},{9,8},{10,9... | collective-permute-start | bytes 393224 | tf_op jit(solution)/shard_map/ppermute | solution.py:20
  217.9 2.8 %copy-start.7 = (bf16[2048,1024]{1,0:T(8,128)(2,1)S(1)}, bf16[2048,1024]{1,0:T(8,128)(2,1)}, u32[]{:S(2)}) copy-start(bf16[2048,1024]{1,0:T(8,128)(2,1)} %all-gather.2.cloned.1.call-done) | copy-start | bytes 12582916
Sparse Core Ops, SparseCore 0:
  100.1 117.7 all-gather.1
